TPU v7x, 256 devices: a 8x8x2 block of a 8x8x16 slice. The times are simulated.
256 devices in a mesh: grp: 2 (over z), sp: 16 (over y, core), tp: 8 (over x).
Axes of the slice: x: 8, y: 8, z: 2, core: 2. Of those that a mesh axis runs over, the one named last changes fastest.
The devices are a block of a 8x8x16 slice.
Arguments:
- resid_in: bfloat16 [32768, 2048], P(('grp', 'sp', 'tp')), parts along dimension 0, may hold values from -6 to 6
- pool_input: bfloat16 [32768, 1024], P(('grp', 'sp'), 'tp'), parts along dimension 0, may hold values from -6 to 6
- pool_weight: bfloat16 [4, 256, 256], replicated, may hold values from -0.375 to 0.375
- pool_scale: float32 [1024], replicated, may hold values from 0.2 to 0.8
- out_weight: bfloat16 [1024, 2048], replicated, may hold values from -0.1875 to 0.1875
- mix_gain: float32 [2048], replicated, may hold values from 0.1 to 1.9
- ffn_gain: float32 [2048], replicated, may hold values from 0.1 to 1.9
- w_gate: bfloat16 [32, 2048, 1024], P('sp', None, 'tp'), may hold values from -0.375 to 0.375
- w_up: bfloat16 [32, 2048, 1024], P('sp', None, 'tp'), may hold values from -0.375 to 0.375
- w_down: bfloat16 [32, 1024, 2048], P('sp', 'tp'), may hold values from -0.1875 to 0.1875
- routes: int32 [32768, 2], P(('grp', 'sp', 'tp')), parts along dimension 0, may hold values from 0 to 31, all different within a row; in each aligned block of 128 rows (0 to 127, 128 to 255, ...) at most 9 rows name the same one
- route_weight: float32 [32768, 2], P(('grp', 'sp', 'tp')), parts along dimension 0, may hold values from 0.1 to 1
- post_gain: float32 [2048], replicated, may hold values from 0.1 to 1.9
Outputs:
- layer_out: bfloat16 [32768, 2048], P(('grp', 'sp', 'tp')), parts along dimension 0
There are 2 independent parts, one for each index of `grp`. A program takes and returns all parts, laid end to end along the dimension named above; an argument that names none is the same for every part. Nothing has to cross between parts.
Inputs may be any that keep to these rules, and one draw needn't show every extreme that they name: `routes`: each row names 2 different experts. The rows of one device name any one expert at most 9 times, and in every draw some device's rows name some expert exactly 9 times.
All inputs are finite; a program needn't handle non-finite values.
Results may differ from a plain program's by a relative error of at most 0.011.
Values may be sent and summed in bfloat16 or wider, within the bound.
A program may use at most 128 MiB of HBM per device.

v0:
```python
import jax
import jax.numpy as jnp
from jax import lax
from jax.sharding import PartitionSpec as P

GROUPS = 4
GROUP_DIM = 256
TOP = 2
CAP = 9
pool_windows = (2, 4, 8, 16)
reach_back = 15
norm_eps = 1e-06
clamp_limit = 7.0
glu_alpha = 1.702


def passed_along(x, axis, by):
    size = lax.axis_size(axis)
    pairs = [(i, i + by) for i in range(size) if 0 <= i + by < size]
    return lax.ppermute(x, axis, pairs)


def rms_scale(values, gain_vec):
    inverse = lax.rsqrt(jnp.mean(values * values, axis=-1, keepdims=True) + norm_eps)
    return values * inverse * gain_vec


def clamped_unit(gate_pre, upward):
    gate_clip = jnp.minimum(gate_pre, clamp_limit)
    linear = jnp.clip(upward, -clamp_limit, clamp_limit)
    return gate_clip * jax.nn.sigmoid(glu_alpha * gate_clip) * (linear + 1.0)


def per_device(
    resid_in,
    pool_input,
    pool_weight,
    pool_scale,
    out_weight,
    mix_gain,
    ffn_gain,
    w_gate,
    w_up,
    w_down,
    routes,
    route_weight,
    post_gain,
):
    n_sp = lax.axis_size("sp")
    n_tp = lax.axis_size("tp")
    seg_rows, channels = pool_input.shape
    last_rows = pool_input[seg_rows - reach_back :]
    before = passed_along(last_rows, "sp", 1)
    extended = jnp.concatenate([before, pool_input], axis=0).astype(jnp.float32)
    first_chan = lax.axis_index("tp") * channels
    chan_group = (first_chan + lax.iota(jnp.int32, channels)) // GROUP_DIM
    positions = lax.axis_index("sp") * seg_rows + lax.iota(jnp.int32, seg_rows)
    window = jnp.zeros((channels,), jnp.int32)
    for group_level, win_len in enumerate(pool_windows):
        window = jnp.where(chan_group == group_level, win_len, window)
    running = jnp.zeros((seg_rows, channels), jnp.float32)
    window_sum = running
    for offset in range(pool_windows[-1]):
        running = running + extended[reach_back - offset : reach_back - offset + seg_rows]
        if offset + 1 in pool_windows:
            window_sum = jnp.where(window[None, :] == offset + 1, running, window_sum)
    divisor = jnp.minimum(positions[:, None] + 1, window[None, :]).astype(jnp.float32)
    mixed_rows = (window_sum / divisor - extended[reach_back:]).astype(jnp.bfloat16)
    token_mixed = lax.all_to_all(mixed_rows, "tp", split_axis=0, concat_axis=1, tiled=True)
    tok_rows = token_mixed.shape[0]
    pooled = jnp.einsum(
        "tgc,gcd->tgd",
        token_mixed.reshape(tok_rows, GROUPS, GROUP_DIM),
        pool_weight,
        preferred_element_type=jnp.float32,
    )
    pooled = (
        (pooled * pool_scale.reshape(GROUPS, GROUP_DIM)).astype(jnp.bfloat16).reshape(tok_rows, -1)
    )
    mix_out = jnp.dot(pooled, out_weight, preferred_element_type=jnp.float32)
    residual = (resid_in.astype(jnp.float32) + rms_scale(mix_out, mix_gain)).astype(jnp.bfloat16)
    normed = rms_scale(residual.astype(jnp.float32), ffn_gain).astype(jnp.bfloat16)
    width = normed.shape[1]
    local_experts = w_gate.shape[0]
    n_experts = local_experts * n_sp
    slot_total = n_experts * CAP
    flat_route = routes.reshape(-1)
    onehot = (flat_route[:, None] == lax.iota(jnp.int32, n_experts)[None, :]).astype(jnp.int32)
    slot_rank = jnp.sum((jnp.cumsum(onehot, axis=0) - onehot) * onehot, axis=1)
    slot_index = flat_route * CAP + slot_rank
    picker = slot_index[:, None] == lax.iota(jnp.int32, slot_total)[None, :]
    picker_rows = picker.astype(jnp.bfloat16)
    token_pick = jnp.sum(
        picker.reshape(tok_rows, TOP, slot_total).astype(jnp.float32), axis=1
    ).astype(jnp.bfloat16)
    buffer = lax.dot_general(
        token_pick, normed, (((0,), (0,)), ((), ())), preferred_element_type=jnp.float32
    )
    outgoing = buffer.astype(jnp.bfloat16).reshape(n_sp, local_experts * CAP, width)
    at_owner = lax.all_to_all(outgoing, "sp", split_axis=0, concat_axis=0, tiled=True)
    arrived = lax.all_gather(at_owner[:, None], "tp", axis=1, tiled=True)
    arrived = arrived.reshape(n_sp, n_tp, local_experts, CAP, width)
    gate_pre = jnp.einsum("sklcd,ldf->sklcf", arrived, w_gate, preferred_element_type=jnp.float32)
    upward = jnp.einsum("sklcd,ldf->sklcf", arrived, w_up, preferred_element_type=jnp.float32)
    activated = clamped_unit(gate_pre, upward).astype(jnp.bfloat16)
    terms = jnp.einsum("sklcf,lfd->kslcd", activated, w_down, preferred_element_type=jnp.float32)
    summed = lax.psum_scatter(
        terms.reshape(1 * lax.axis_size("tp"), n_sp, local_experts * CAP, width).astype(
            jnp.bfloat16
        ),
        "tp",
        scatter_dimension=0,
        tiled=True,
    ).astype(jnp.float32)
    results = summed[0].astype(jnp.bfloat16)
    returned = lax.all_to_all(results, "sp", split_axis=0, concat_axis=0, tiled=True).reshape(
        slot_total, width
    )
    gathered = jnp.dot(picker_rows, returned, preferred_element_type=jnp.float32)
    expert_mix = jnp.sum(gathered.reshape(tok_rows, TOP, width) * route_weight[:, :, None], axis=1)
    return (residual.astype(jnp.float32) + rms_scale(expert_mix, post_gain)).astype(jnp.bfloat16)


def solution(mesh):
    in_specs = (
        P(("grp", "sp", "tp"), None),
        P(("grp", "sp"), "tp"),
        P(),
        P(),
        P(),
        P(),
        P(),
        P("sp", None, "tp"),
        P("sp", None, "tp"),
        P("sp", "tp", None),
        P(("grp", "sp", "tp"), None),
        P(("grp", "sp", "tp"), None),
        P(),
    )
    out_specs = P(("grp", "sp", "tp"), None)
    return jax.shard_map(
        per_device, mesh=mesh, in_specs=in_specs, out_specs=out_specs, check_vma=False
    )
```

profile of v0, /device:TPU:513, one launch (start us, length us, event | category | flops | bytes accessed | tf_op | source)
XLA Modules:
  0.0 397.1 jit_solution(8766756153125260866)
XLA Ops:
  7.3 5.7 %collective-permute-start = (bf16[15,128]{1,0:T(8,128)(2,1)S(1)}, bf16[15,128]{1,0:T(8,128)(2,1)S(1)}, u32[]{:S(2)}, u32[]{:S(2)}) collective-permute-start(bf16[15,128]{1,0:T(8,128)(2,1)S(1)} %slice.58), channel_id=1, source_target_pairs={{0,8},{8,16},{16,24},{24,32},{32,40},{40,48},{48,56},{56,64},{64,7... | collective-permute-start | bytes 11528 | tf_op jit(solution)/shard_map/ppermute | solution.py:20
  13.1 0.8 copy.76
  14.7 15.0 %collective-permute-done = bf16[15,128]{1,0:T(8,128)(2,1)S(1)} collective-permute-done((bf16[15,128]{1,0:T(8,128)(2,1)S(1)}, bf16[15,128]{1,0:T(8,128)(2,1)S(1)}, u32[]{:S(2)}, u32[]{:S(2)}) %collective-permute-start) | collective-permute-done | bytes 3872 | tf_op jit(solution)/shard_map/ppermute | solution.py:20
  29.7 1.0 maximum_convert_fusion
  30.7 1.5 fusion.42
  32.2 3.7 all-to-all-start
  36.8 9.4 %all-to-all-done = bf16[8,128,128]{2,1,0:T(8,128)(2,1)S(1)} async-done(((bf16[8,128,128]{2,1,0:T(8,128)(2,1)}), bf16[8,128,128]{2,1,0:T(8,128)(2,1)S(1)}, u32[]{:S(2)}, u32[]{:S(2)}) %all-to-all-start) | async-done | bytes 262176 | tf_op jit(solution)/shard_map/all_to_all | solution.py:69
  46.9 3.1 multiply_reduce_fusion.1
  50.7 1.6 convolution_convert_fusion
  52.2 1.4 reshape.162
  53.7 44.4 %all_to_all.26 = bf16[16,18,2048]{2,1,0:T(8,128)(2,1)S(1)} all-to-all(bf16[16,18,2048]{2,1,0:T(8,128)(2,1)S(1)} %reshape.162), channel_id=1, replica_groups=mesh['grp'=2,'sp'=16,'tp'=8] {'sp'}, dimensions={0} | all-to-all | bytes 2359296 | tf_op jit(solution)/shard_map/all_to_all | solution.py:100
  98.1 1.7 copy.80
  100.1 104.1 %all-gather.3.cloned.1.call-done = bf16[16,144,2048]{2,0,1:T(8,128)(2,1)} async-done(((bf16[16,18,2048]{2,0,1:T(8,128)(2,1)}), bf16[16,144,2048]{2,0,1:T(8,128)(2,1)}) %all-gather.3.cloned.1.call-update) | async-done | bytes 9437200 | tf_op jit(solution)/shard_map/all_gather | solution.py:101
  204.2 5.3 %fusion.20 = f32[16,8,2,9,128]{4,0,3,1,2:T(8,128)S(1)} fusion(bf16[16,8,2,9,2048]{4,0,3,2,1:T(8,128)(2,1)} %bitcast.67, bf16[2,2048,128]{2,1,0:T(8,128)(2,1)S(1)} %copy-done.9), kind=kOutput, calls=%fused_computation.16 | convolution fusion | flops 1208254464 | bytes 11665408 | tf_op jit(solution)/shard_map/sklcd,ldf->sklcf/dot_general | solution.py:103
  209.5 1.1 copy-done.8
  210.9 2.8 fusion.23
  213.7 5.1 %convert_bitcast_fusion = bf16[8,16,2,9,2048]{4,0,3,1,2:T(8,128)(2,1)} fusion(bf16[2,128,2048]{2,1,0:T(8,128)(2,1)S(1)} %copy-done, bf16[16,8,2,9,128]{4,0,3,1,2:T(8,128)(2,1)S(1)} %fusion.23), kind=kOutput, calls=%fused_computation | convolution fusion | flops 1212678144 | bytes 11075584 | tf_op jit(solution)/shard_map/sklcf,lfd->kslcd/dot_general | solution.py:106
  218.8 12.5 %copy.84 = bf16[8,16,2,9,2048]{4,1,3,2,0:T(8,128)(2,1)} copy(bf16[8,16,2,9,2048]{4,0,3,1,2:T(8,128)(2,1)} %convert_bitcast_fusion) | data formatting | bytes 18874368 | tf_op jit(solution)/shard_map/convert_element_type | solution.py:108
  231.3 105.1 %reduce-scatter.2.cloned.1.call-done = bf16[1,16,18,2048]{3,1,2,0:T(8,128)(2,1)} async-done(((bf16[8,16,18,2048]{3,1,2,0:T(8,128)(2,1)}), bf16[1,16,18,2048]{3,1,2,0:T(8,128)(2,1)}) %reduce-scatter.2.cloned.1.call-update) | async-done | bytes 1179664 | tf_op jit(solution)/shard_map/reduce_scatter | solution.py:107
  336.5 2.0 copy.85
  338.5 47.2 %all_to_all.27 = bf16[16,18,2048]{2,1,0:T(8,128)(2,1)S(1)} all-to-all(bf16[16,18,2048]{2,1,0:T(8,128)(2,1)S(1)} %copy.85), channel_id=1, replica_groups=mesh['grp'=2,'sp'=16,'tp'=8] {'sp'}, dimensions={0} | all-to-all | bytes 2359296 | tf_op jit(solution)/shard_map/all_to_all | solution.py:116
  385.7 1.2 reshape.170
  386.9 2.1 fusion.4
  389.2 1.0 fusion.31
  (53 shorter events, 4.5 us)
Async XLA Ops:
  6.5 207.2 %copy-start = (bf16[2,128,2048]{2,1,0:T(8,128)(2,1)S(1)}, bf16[2,128,2048]{2,1,0:T(8,128)(2,1)}, u32[]{:S(2)}) copy-start(bf16[2,128,2048]{2,1,0:T(8,128)(2,1)} %param.22) | copy-start | bytes 3145732
  7.3 22.4 %collective-permute-start = (bf16[15,128]{1,0:T(8,128)(2,1)S(1)}, bf16[15,128]{1,0:T(8,128)(2,1)S(1)}, u32[]{:S(2)}, u32[]{:S(2)}) collective-permute-start(bf16[15,128]{1,0:T(8,128)(2,1)S(1)} %slice.58), channel_id=1, source_target_pairs={{0,8},{8,16},{16,24},{24,32},{32,40},{40,48},{48,56},{56,64},{64,7... | collective-permute-start | bytes 11528 | tf_op jit(solution)/shard_map/ppermute | solution.py:20
  30.7 5.7 %copy-start.7 = (f32[1024]{0:T(1024)S(1)}, f32[1024]{0:T(1024)}, u32[]{:S(2)}) copy-start(f32[1024]{0:T(1024)} %param.16) | copy-start | bytes 12292
  30.7 6.0 %copy-start.6 = (s32[128,2]{0,1:T(2,128)S(1)}, s32[128,2]{0,1:T(2,128)}, u32[]{:S(2)}) copy-start(s32[128,2]{0,1:T(2,128)} %param.23) | copy-start | bytes 3076
  32.2 14.2 %copy-start.1 = (bf16[4,256,256]{2,1,0:T(8,128)(2,1)S(1)}, bf16[4,256,256]{2,1,0:T(8,128)(2,1)}, u32[]{:S(2)}) copy-start(bf16[4,256,256]{2,1,0:T(8,128)(2,1)} %param.15) | copy-start | bytes 1572868
  32.2 14.0 %all-to-all-start = ((bf16[8,128,128]{2,1,0:T(8,128)(2,1)}), bf16[8,128,128]{2,1,0:T(8,128)(2,1)S(1)}, u32[]{:S(2)}, u32[]{:S(2)}) async-start(bf16[8,128,128]{2,1,0:T(8,128)(2,1)} %bitcast), calls=%async_computation | async-start | bytes 524288 | tf_op jit(solution)/shard_map/all_to_all | solution.py:69
  36.0 168.2 %all-gather.3.cloned.1.call-start = ((), (), s32[]{:S(2)}) async-start(), calls=%async_computation.5 | async-start | bytes 10616832 | tf_op jit(solution)/shard_map/all_gather | solution.py:101
  46.9 3.1 copy-start.2
  46.9 3.1 copy-start.3
  50.0 0.7 copy-start.4
  99.8 104.4 %copy-start.9 = (bf16[2,2048,128]{2,1,0:T(8,128)(2,1)S(1)}, bf16[2,2048,128]{2,1,0:T(8,128)(2,1)}, u32[]{:S(2)}) copy-start(bf16[2,2048,128]{2,1,0:T(8,128)(2,1)} %param.20) | copy-start | bytes 3145732
  99.8 236.6 %reduce-scatter.2.cloned.1.call-start = ((), (), s32[]{:S(2)}) async-start(), calls=%async_computation.4 | async-start | bytes 10616832 | tf_op jit(solution)/shard_map/reduce_scatter | solution.py:107
  204.2 6.4 %copy-start.8 = (bf16[16,144,2048]{2,0,1:T(8,128)(2,1)S(1)}, bf16[16,144,2048]{2,0,1:T(8,128)(2,1)}, u32[]{:S(2)}) copy-start(bf16[16,144,2048]{2,0,1:T(8,128)(2,1)} %all-gather.3.cloned.1.call-done) | copy-start | bytes 28311556
  204.2 6.7 %copy-start.10 = (bf16[2,2048,128]{2,1,0:T(8,128)(2,1)S(1)}, bf16[2,2048,128]{2,1,0:T(8,128)(2,1)}, u32[]{:S(2)}) copy-start(bf16[2,2048,128]{2,1,0:T(8,128)(2,1)} %param.21) | copy-start | bytes 3145732
  385.7 1.2 copy-start.11
  386.9 2.3 copy-start.5
Sparse Core Ops, SparseCore 0:
  100.0 104.1 all-gather.2
  231.5 104.9 reduce-scatter.1
where the time goes:
time: 398 us; the launch traced here: 397 us
  waiting for transfers between devices  234 us (59%)
  blocking collectives  91.7 us (23%)
  local copies, waits for them, and re-layouts  23 us (6%)
  matrix products  20.2 us (5%)
  between operations  13.7 us (3%)
  starting transfers between devices  9.79 us (2%)
  other arithmetic  4.91 us (1%)
    reduce_scatter x1, waiting for transfers between devices, per_device(): lax.psum_scatter(terms.reshape(1 * lax.axis_size('tp'), n_sp, local_exper...  105 us
    all_gather x1, waiting for transfers between devices, per_device(): arrived = lax.all_gather(at_owner[:, None], 'tp', axis=1, tiled=True)  104 us
    all_to_all x1, blocking collectives, per_device(): lax.all_to_all(results, 'sp', split_axis=0, concat_axis=0, tiled=True)  47.2 us
    all_to_all x1, blocking collectives, per_device(): lax.all_to_all(outgoing, 'sp', split_axis=0, concat_axis=0, tiled=True)  44.4 us
    ppermute x1, waiting for transfers between devices, passed_along(): return lax.ppermute(x, axis, pairs)  15 us
    convert_element_type x1, local copies, waits for them, and re-layouts, per_device(): terms.reshape(1 * lax.axis_size('tp'), n_sp, local_experts * CAP, width)  12.5 us
    all_to_all x1, waiting for transfers between devices, per_device(): lax.all_to_all(mixed_rows, 'tp', split_axis=0, concat_axis=1, tiled=True)  9.42 us
  transfers between devices with their start and end apart: 4, of which 4 were waited for; matrix products, arithmetic and copies ran while one was open for 1% of the time, Pallas kernels for 0%

commit v1 on v0

--- a/solution.py
+++ b/solution.py
@@ -98,7 +98,9 @@
     )
     outgoing = buffer.astype(jnp.bfloat16).reshape(n_sp, local_experts * CAP, width)
     at_owner = lax.all_to_all(outgoing, "sp", split_axis=0, concat_axis=0, tiled=True)
-    arrived = lax.all_gather(at_owner[:, None], "tp", axis=1, tiled=True)
+    arrived = jnp.concatenate(
+        lax.all_to_all(jnp.stack([at_owner[:, None]] * lax.axis_size("tp")), "tp", 0, 0), axis=1
+    )
     arrived = arrived.reshape(n_sp, n_tp, local_experts, CAP, width)
     gate_pre = jnp.einsum("sklcd,ldf->sklcf", arrived, w_gate, preferred_element_type=jnp.float32)
     upward = jnp.einsum("sklcd,ldf->sklcf", arrived, w_up, preferred_element_type=jnp.float32)

time: 398 us -> 525 us (1.32)
  blocking collectives: 91.7 us -> 304 us
  waiting for transfers between devices: 234 us -> 131 us
  matrix products: 20.2 us -> 39.3 us
    all_to_all x0 -> x1, blocking collectives: none -> 212 us  [per_device(): lax.all_to_all(jnp.stack([at_owner[:, None]] * lax.axis_size('tp')), 'tp'...]
    all_gather x1 -> x0, waiting for transfers between devices: 104 us -> none  [per_device(): arrived = lax.all_gather(at_owner[:, None], 'tp', axis=1, tiled=True)]
    dot_general x1, matrix products: 2.82 us -> 15.7 us  [per_device(): jnp.einsum('sklcd,ldf->sklcf', arrived, w_up, preferred_element_type=jnp....]
    dot_general x1, matrix products: 5.33 us -> 11.3 us  [per_device(): jnp.einsum('sklcd,ldf->sklcf', arrived, w_gate, preferred_element_type=jn...]
  transfers between devices with their start and end apart: 4 -> 3, of which waited for: 4 -> 3; matrix products, arithmetic and copies ran while one was open for 1% -> 0% of each run, Pallas kernels for 0% -> 0%
where the time goes in v1:
time: 525 us; the launch traced here: 524 us
  blocking collectives  304 us (58%)
  waiting for transfers between devices  131 us (25%)
  matrix products  39.3 us (7%)
  local copies, waits for them, and re-layouts  21.9 us (4%)
  between operations  13.7 us (3%)
  starting transfers between devices  9.55 us (2%)
  other arithmetic  5.53 us (1%)
    all_to_all x1, blocking collectives, per_device(): lax.all_to_all(jnp.stack([at_owner[:, None]] * lax.axis_size('tp')), 'tp'...  212 us
    reduce_scatter x1, waiting for transfers between devices, per_device(): lax.psum_scatter(terms.reshape(1 * lax.axis_size('tp'), n_sp, local_exper...  106 us
    all_to_all x1, blocking collectives, per_device(): lax.all_to_all(results, 'sp', split_axis=0, concat_axis=0, tiled=True)  47.2 us
    all_to_all x1, blocking collectives, per_device(): lax.all_to_all(outgoing, 'sp', split_axis=0, concat_axis=0, tiled=True)  44.4 us
    dot_general x1, matrix products, per_device(): jnp.einsum('sklcd,ldf->sklcf', arrived, w_up, preferred_element_type=jnp....  15.7 us
    ppermute x1, waiting for transfers between devices, passed_along(): return lax.ppermute(x, axis, pairs)  15 us
    convert_element_type x1, local copies, waits for them, and re-layouts, per_device(): terms.reshape(1 * lax.axis_size('tp'), n_sp, local_experts * CAP, width)  12.5 us
    dot_general x1, matrix products, per_device(): jnp.einsum('sklcd,ldf->sklcf', arrived, w_gate, preferred_element_type=jn...  11.3 us
  transfers between devices with their start and end apart: 3, of which 3 were waited for; matrix products, arithmetic and copies ran while one was open for 0% of the time, Pallas kernels for 0%

profile of v1, /device:TPU:513, one launch (start us, length us, event | category | flops | bytes accessed | tf_op | source)
XLA Modules:
  0.0 524.2 jit_solution(4070096951398227373)
XLA Ops:
  6.6 0.8 slice.58
  7.3 5.7 %collective-permute-start = (bf16[15,128]{1,0:T(8,128)(2,1)S(1)}, bf16[15,128]{1,0:T(8,128)(2,1)S(1)}, u32[]{:S(2)}, u32[]{:S(2)}) collective-permute-start(bf16[15,128]{1,0:T(8,128)(2,1)S(1)} %slice.58), channel_id=1, source_target_pairs={{0,8},{8,16},{16,24},{24,32},{32,40},{40,48},{48,56},{56,64},{64,7... | collective-permute-start | bytes 11528 | tf_op jit(solution)/shard_map/ppermute | solution.py:20
  13.1 0.8 copy.89
  14.7 15.0 %collective-permute-done = bf16[15,128]{1,0:T(8,128)(2,1)S(1)} collective-permute-done((bf16[15,128]{1,0:T(8,128)(2,1)S(1)}, bf16[15,128]{1,0:T(8,128)(2,1)S(1)}, u32[]{:S(2)}, u32[]{:S(2)}) %collective-permute-start) | collective-permute-done | bytes 3872 | tf_op jit(solution)/shard_map/ppermute | solution.py:20
  29.7 1.0 maximum_convert_fusion
  30.7 1.5 fusion.27
  32.2 3.7 all-to-all-start
  36.8 9.4 %all-to-all-done = bf16[8,128,128]{2,1,0:T(8,128)(2,1)S(1)} async-done(((bf16[8,128,128]{2,1,0:T(8,128)(2,1)}), bf16[8,128,128]{2,1,0:T(8,128)(2,1)S(1)}, u32[]{:S(2)}, u32[]{:S(2)}) %all-to-all-start) | async-done | bytes 262176 | tf_op jit(solution)/shard_map/all_to_all | solution.py:69
  46.9 3.1 multiply_reduce_fusion.1
  50.7 1.6 convolution_convert_fusion
  52.2 1.4 reshape.164
  53.7 44.4 %all_to_all.31 = bf16[16,18,2048]{2,1,0:T(8,128)(2,1)S(1)} all-to-all(bf16[16,18,2048]{2,1,0:T(8,128)(2,1)S(1)} %reshape.164), channel_id=1, replica_groups=mesh['grp'=2,'sp'=16,'tp'=8] {'sp'}, dimensions={0} | all-to-all | bytes 2359296 | tf_op jit(solution)/shard_map/all_to_all | solution.py:100
  98.8 1.2 stack.3
  100.0 212.1 %all_to_all.32 = bf16[8,16,1,18,2048]{4,1,3,2,0:T(8,128)(2,1)} all-to-all(bf16[8,16,1,18,2048]{4,1,3,2,0:T(8,128)(2,1)S(1)} %stack.3), channel_id=1, replica_groups=mesh['grp'=2,'sp'=16,'tp'=8] {'tp'}, dimensions={0} | all-to-all | bytes 18874368 | tf_op jit(solution)/shard_map/all_to_all | solution.py:102
  312.0 15.7 %fusion = f32[2,16,8,9,128]{4,2,3,1,0:T(8,128)S(1)} fusion(bf16[16,8,2,9,2048]{4,0,3,2,1:T(8,128)(2,1)} %bitcast.78, bf16[2,2048,128]{2,1,0:T(8,128)(2,1)S(1)} %copy-done.9), kind=kOutput, calls=%fused_computation.1 | convolution fusion | flops 1207959552 | bytes 11665408 | tf_op jit(solution)/shard_map/sklcd,ldf->sklcf/dot_general | solution.py:106
  327.7 11.3 %fusion.2 = f32[2,16,8,9,128]{4,2,3,1,0:T(8,128)S(1)} fusion(bf16[16,8,2,9,2048]{4,0,3,2,1:T(8,128)(2,1)S(1)} %bitcast.79, bf16[2,2048,128]{2,1,0:T(8,128)(2,1)} %param.20), kind=kOutput, calls=%fused_computation.3 | convolution fusion | flops 1207959552 | bytes 11665408 | tf_op jit(solution)/shard_map/sklcd,ldf->sklcf/dot_general | solution.py:105
  339.7 5.3 %convert_bitcast_fusion = bf16[8,16,2,9,2048]{4,0,3,1,2:T(8,128)(2,1)} fusion(bf16[2,128,2048]{2,1,0:T(8,128)(2,1)S(1)} %copy-done, bf16[16,8,2,9,128]{4,0,3,1,2:T(8,128)(2,1)S(1)} %fusion.6), kind=kOutput, calls=%fused_computation | convolution fusion | flops 1212678144 | bytes 11075584 | tf_op jit(solution)/shard_map/sklcf,lfd->kslcd/dot_general | solution.py:108
  345.0 12.5 %copy.98 = bf16[8,16,2,9,2048]{4,1,3,2,0:T(8,128)(2,1)} copy(bf16[8,16,2,9,2048]{4,0,3,1,2:T(8,128)(2,1)} %convert_bitcast_fusion) | data formatting | bytes 18874368 | tf_op jit(solution)/shard_map/convert_element_type | solution.py:110
  357.6 106.1 %reduce-scatter.2.cloned.1.call-done = bf16[1,16,18,2048]{3,1,2,0:T(8,128)(2,1)} async-done(((bf16[8,16,18,2048]{3,1,2,0:T(8,128)(2,1)}), bf16[1,16,18,2048]{3,1,2,0:T(8,128)(2,1)}) %reduce-scatter.2.cloned.1.call-update) | async-done | bytes 1179664 | tf_op jit(solution)/shard_map/reduce_scatter | solution.py:109
  463.6 2.0 copy.99
  465.6 47.2 %all_to_all.33 = bf16[16,18,2048]{2,1,0:T(8,128)(2,1)S(1)} all-to-all(bf16[16,18,2048]{2,1,0:T(8,128)(2,1)S(1)} %copy.99), channel_id=1, replica_groups=mesh['grp'=2,'sp'=16,'tp'=8] {'sp'}, dimensions={0} | all-to-all | bytes 2359296 | tf_op jit(solution)/shard_map/all_to_all | solution.py:118
  512.8 1.2 reshape.170
  514.0 2.1 fusion.4
  516.3 1.0 fusion.16
  (51 shorter events, 4.4 us)
Async XLA Ops:
  6.5 333.1 %copy-start = (bf16[2,128,2048]{2,1,0:T(8,128)(2,1)S(1)}, bf16[2,128,2048]{2,1,0:T(8,128)(2,1)}, u32[]{:S(2)}) copy-start(bf16[2,128,2048]{2,1,0:T(8,128)(2,1)} %param.22) | copy-start | bytes 3145732
  7.3 22.4 %collective-permute-start = (bf16[15,128]{1,0:T(8,128)(2,1)S(1)}, bf16[15,128]{1,0:T(8,128)(2,1)S(1)}, u32[]{:S(2)}, u32[]{:S(2)}) collective-permute-start(bf16[15,128]{1,0:T(8,128)(2,1)S(1)} %slice.58), channel_id=1, source_target_pairs={{0,8},{8,16},{16,24},{24,32},{32,40},{40,48},{48,56},{56,64},{64,7... | collective-permute-start | bytes 11528 | tf_op jit(solution)/shard_map/ppermute | solution.py:20
  30.7 5.7 %copy-start.8 = (f32[1024]{0:T(1024)S(1)}, f32[1024]{0:T(1024)}, u32[]{:S(2)}) copy-start(f32[1024]{0:T(1024)} %param.16) | copy-start | bytes 12292
  30.7 6.0 %copy-start.7 = (s32[128,2]{0,1:T(2,128)S(1)}, s32[128,2]{0,1:T(2,128)}, u32[]{:S(2)}) copy-start(s32[128,2]{0,1:T(2,128)} %param.23) | copy-start | bytes 3076
  32.2 14.2 %copy-start.2 = (bf16[4,256,256]{2,1,0:T(8,128)(2,1)S(1)}, bf16[4,256,256]{2,1,0:T(8,128)(2,1)}, u32[]{:S(2)}) copy-start(bf16[4,256,256]{2,1,0:T(8,128)(2,1)} %param.15) | copy-start | bytes 1572868
  32.2 14.0 %all-to-all-start = ((bf16[8,128,128]{2,1,0:T(8,128)(2,1)}), bf16[8,128,128]{2,1,0:T(8,128)(2,1)S(1)}, u32[]{:S(2)}, u32[]{:S(2)}) async-start(bf16[8,128,128]{2,1,0:T(8,128)(2,1)} %bitcast), calls=%async_computation | async-start | bytes 524288 | tf_op jit(solution)/shard_map/all_to_all | solution.py:69
  36.0 427.7 %reduce-scatter.2.cloned.1.call-start = ((), (), s32[]{:S(2)}) async-start(), calls=%async_computation.5 | async-start | bytes 10616832 | tf_op jit(solution)/shard_map/reduce_scatter | solution.py:109
  46.9 3.1 copy-start.3
  46.9 3.1 copy-start.4
  50.0 0.7 copy-start.5
  100.0 212.1 %copy-start.9 = (bf16[2,2048,128]{2,1,0:T(8,128)(2,1)S(1)}, bf16[2,2048,128]{2,1,0:T(8,128)(2,1)}, u32[]{:S(2)}) copy-start(bf16[2,2048,128]{2,1,0:T(8,128)(2,1)} %param.21) | copy-start | bytes 3145732
  312.0 15.7 %copy-start.1 = (bf16[8,16,1,18,2048]{4,1,3,2,0:T(8,128)(2,1)S(1)}, bf16[8,16,1,18,2048]{4,1,3,2,0:T(8,128)(2,1)}, u32[]{:S(2)}) copy-start(bf16[8,16,1,18,2048]{4,1,3,2,0:T(8,128)(2,1)} %all_to_all.32) | copy-start | bytes 28311556
  512.8 1.2 copy-start.10
  514.0 2.3 copy-start.6
Sparse Core Ops, SparseCore 0:
  357.7 105.8 reduce-scatter.1
